TPU v7x, 32 devices: a whole 2x2x4 slice. The times are simulated.
32 devices in a mesh: grp: 2 (over y), dp: 2 (over x), kv: 4 (over z), tp: 2 (over core).
Axes of the slice: x: 2, y: 2, z: 4, core: 2. Of those that a mesh axis runs over, the one named last changes fastest.
Arguments:
- queries: bfloat16 [4, 1024, 2048], P(('grp', 'dp'), 'kv', 'tp'), parts along dimension 0, may hold values from -10 to 10
- keys: bfloat16 [4, 1024, 512], P(('grp', 'dp'), 'kv', 'tp'), parts along dimension 0, may hold values from -10 to 10
- values: bfloat16 [4, 1024, 512], P(('grp', 'dp'), 'kv', 'tp'), parts along dimension 0, may hold values from -6 to 6
- gate_logits: float32 [4, 2, 1024, 32], P(('grp', 'dp'), None, 'kv', 'tp'), parts along dimension 0, may hold values from -6 to 6
- chosen: int32 [4, 8, 8, 16], P(('grp', 'dp'), 'kv', 'tp'), parts along dimension 0, may hold values from -1 to 15, as said below
- pool_k: float32 [32, 64], replicated, may hold values from 0 to 0.35
- pool_v: float32 [32, 64], replicated, may hold values from 0 to 0.35
- out_gain: float32 [2048], P('tp'), may hold values from 0.1 to 1.9
Outputs:
- attended: bfloat16 [4, 1024, 2048], P(('grp', 'dp'), 'kv', 'tp'), parts along dimension 0
There are 2 independent parts, one for each index of `grp`. A program takes and returns all parts, laid end to end along the dimension named above; an argument that names none is the same for every part. Nothing has to cross between parts.
Inputs may be any that keep to these rules, and one draw needn't show every extreme that they name: Entries are key block numbers (block e holds positions e * 64 to e * 64 + 63) or -1 for none. The list of query block b (positions b * 128 onward) holds the blocks that contain its own positions, other distinct blocks that begin before it, and -1 in its remaining entries. For the query blocks of one span of 256 positions and one key head, the blocks chosen from any other span number at most 2; in every draw some span reaches 2.
All inputs are finite; a program needn't handle non-finite values.
Results may differ from a plain program's by a relative error of at most 0.0079.
Values may be sent and summed in bfloat16 or wider, within the bound.
A program may use at most 64 MiB of HBM per device.

v0:
```python
import jax
import jax.numpy as jnp
from jax import lax
from jax.sharding import PartitionSpec as P

DH = 64
CMP_STRIDE = 16
CMP_BLOCK = 32
SLC = 64
QB = 128
NSEL = 16
MOST = 2


THETA = 500000.0
EPS = 1e-06
NEG = -1e30


def shifted(block, axis, distance):
    devices = range(lax.axis_size(axis))
    route = [(i - distance, i) for i in devices if i - distance in devices]
    return lax.ppermute(block, axis, route)


def rotate(matrix, start, heads):
    length = matrix.shape[0]
    half = DH // 2
    place = (start + jnp.arange(length)).astype(jnp.float32)
    freq = jnp.power(jnp.float32(THETA), -(2.0 * jnp.arange(half).astype(jnp.float32)) / DH)
    angle = place[:, None] * freq[None, :]
    cosine = jnp.cos(angle)[:, None, :]
    sine = jnp.sin(angle)[:, None, :]
    parts = matrix.reshape(length, heads, DH).astype(jnp.float32)
    first = parts[..., :half]
    second = parts[..., half:]
    turned = jnp.concatenate([first * cosine - second * sine, second * cosine + first * sine], -1)
    return turned.reshape(length, heads * DH).astype(jnp.bfloat16)


def compress(extended, pool, groups):
    count = extended.shape[0] // CMP_STRIDE - 1
    parts = extended.reshape(count + 1, CMP_STRIDE, groups, DH).astype(jnp.float32)
    lower = jnp.einsum(
        "nigd,id->ngd", parts[:-1], pool[:CMP_STRIDE], precision=lax.Precision.HIGHEST
    )
    upper = jnp.einsum(
        "nigd,id->ngd", parts[1:], pool[CMP_STRIDE:], precision=lax.Precision.HIGHEST
    )
    return (lower + upper).astype(jnp.bfloat16)


def wanted_blocks(lists, owners, per_owner):
    groups = lists.shape[1]
    total = owners * per_owner
    hits = lists[..., None] == jnp.arange(total, dtype=jnp.int32)
    member = jnp.any(hits, axis=(0, 2)).astype(jnp.int32).reshape(groups, owners, per_owner)
    rank = jnp.cumsum(member, -1) - member
    slot_hit = (member[..., None] == 1) & (rank[..., None] == jnp.arange(MOST))
    local_ids = jnp.arange(per_owner, dtype=jnp.int32)[:, None]
    asked = jnp.sum(jnp.where(slot_hit, local_ids, 0), axis=2)
    return (asked.transpose(1, 0, 2), rank.reshape(groups, total))


def per_device(queries, keys, values, gate_logits, chosen, pool_k, pool_v, out_gain):
    queries = queries[0]
    keys = keys[0]
    values = values[0]
    logits = gate_logits[0]
    lists = chosen[0]
    length = queries.shape[0]
    groups = keys.shape[1] // DH
    heads = queries.shape[1] // DH
    per_group = heads // groups
    qblocks = length // QB
    owners = lax.axis_size("kv")
    myself = lax.axis_index("kv")
    start = myself * length
    scale = DH ** (-0.5)
    query_turned = rotate(queries, start, heads)
    key_turned = rotate(keys, start, groups)
    next_keys, next_values = shifted((keys[:CMP_STRIDE], values[:CMP_STRIDE]), "kv", -1)
    key_summary = compress(jnp.concatenate([keys, next_keys], 0), pool_k, groups)
    value_summary = compress(jnp.concatenate([values, next_values], 0), pool_v, groups)
    place = start + jnp.arange(length)
    query_group = queries.reshape(length, groups, per_group, DH).transpose(1, 2, 0, 3)
    part_keys = lax.all_gather(key_summary, "kv", axis=0, tiled=True)
    part_values = lax.all_gather(value_summary, "kv", axis=0, tiled=True)
    count = part_keys.shape[0]
    ends = jnp.arange(count) * CMP_STRIDE + CMP_BLOCK - 1
    allow = ends[None, :] <= place[:, None]

    def per_group_fold(item):
        query_part, key_part, value_part, top, total, summed = item
        score = (
            jnp.einsum("htd,nd->htn", query_part, key_part, preferred_element_type=jnp.float32)
            * scale
        )
        score = jnp.where(allow, score, NEG)
        fresh = jnp.maximum(top, jnp.max(score, -1))
        weight = jnp.where(allow, jnp.exp(score - fresh[..., None]), 0.0)
        shrink = jnp.exp(top - fresh)
        total = total * shrink + jnp.sum(weight, -1)
        summed = summed * shrink[..., None] + jnp.einsum(
            "htn,nd->htd",
            weight.astype(jnp.bfloat16),
            value_part,
            preferred_element_type=jnp.float32,
        )
        return (fresh, total, summed)

    top = jnp.full((groups, per_group, length), NEG, jnp.float32)
    total = jnp.zeros((groups, per_group, length), jnp.float32)
    summed = jnp.zeros((groups, per_group, length, DH), jnp.float32)
    top, total, summed = lax.map(
        per_group_fold,
        (
            query_group,
            part_keys.transpose(1, 0, 2),
            part_values.transpose(1, 0, 2),
            top,
            total,
            summed,
        ),
    )
    summary_out = summed / jnp.maximum(total, 1.0)[..., None]
    group_pick = jnp.arange(groups)[None, :, None]
    safe = jnp.maximum(lists, 0)
    per_owner = length // SLC
    asked_ids, rank = wanted_blocks(lists, owners, per_owner)
    requests = lax.all_to_all(asked_ids, "kv", split_axis=0, concat_axis=0, tiled=True)
    local_keys = key_turned.reshape(per_owner, SLC, groups, DH)
    local_values = values.reshape(per_owner, SLC, groups, DH)
    served = (local_keys[requests, :, group_pick, :], local_values[requests, :, group_pick, :])
    got_keys, got_values = (
        lax.all_to_all(served[0], "kv", split_axis=0, concat_axis=0, tiled=True),
        lax.all_to_all(served[1], "kv", split_axis=0, concat_axis=0, tiled=True),
    )

    def table(received, local):
        remote = received.transpose(1, 0, 2, 3, 4).reshape(groups, owners * MOST, SLC, DH)
        return jnp.concatenate([remote, local.transpose(2, 0, 1, 3)], 1)

    owner = safe // per_owner
    inner = safe % per_owner
    slot = jnp.where(owner == myself, owners * MOST + inner, owner * MOST + rank[group_pick, safe])
    key_sel = table(got_keys, local_keys)[group_pick, slot]
    value_sel = table(got_values, local_values)[group_pick, slot]
    query_blocks = query_turned.reshape(qblocks, QB, groups, per_group, DH)

    def attend(item):
        index, query_part, keys_part, values_part, picks = item
        place_q = start + index * QB + jnp.arange(QB)
        score = jnp.einsum(
            "tghd,gnkd->ghtnk", query_part, keys_part, preferred_element_type=jnp.float32
        )
        score = score.reshape(groups, per_group, QB, NSEL * SLC) * scale
        safe_picks = jnp.maximum(picks, 0)
        key_place = (safe_picks[..., None] * SLC + jnp.arange(SLC)).reshape(groups, NSEL * SLC)
        live = jnp.broadcast_to(picks[..., None] >= 0, (groups, NSEL, SLC)).reshape(
            groups, NSEL * SLC
        )
        allow = (live[:, None, :] & (key_place[:, None, :] <= place_q[None, :, None]))[:, None]
        score = jnp.where(allow, score, NEG)
        top_sel = jnp.max(score, -1, keepdims=True)
        weight = jnp.where(allow, jnp.exp(score - top_sel), 0.0)
        total_sel = jnp.sum(weight, -1)
        flat_values = values_part.reshape(groups, NSEL * SLC, DH)
        out = jnp.einsum(
            "ghtk,gkd->ghtd",
            weight.astype(jnp.bfloat16),
            flat_values,
            preferred_element_type=jnp.float32,
        )
        return out / total_sel[..., None]

    chosen_out = lax.map(attend, (jnp.arange(qblocks), query_blocks, key_sel, value_sel, lists))
    gates = jax.nn.sigmoid(logits)
    summary_rows = summary_out.transpose(2, 0, 1, 3).reshape(length, heads, DH)
    chosen_rows = chosen_out.transpose(0, 3, 1, 2, 4).reshape(length, heads, DH)
    mixed = gates[0][..., None] * summary_rows + gates[1][..., None] * chosen_rows
    normed = (
        mixed
        * lax.rsqrt(jnp.mean(mixed * mixed, -1, keepdims=True) + EPS)
        * out_gain.reshape(heads, DH)
    )
    return normed.reshape(1, length, heads * DH).astype(jnp.bfloat16)


def solution(mesh):
    in_specs = (
        P(("grp", "dp"), "kv", "tp"),
        P(("grp", "dp"), "kv", "tp"),
        P(("grp", "dp"), "kv", "tp"),
        P(("grp", "dp"), None, "kv", "tp"),
        P(("grp", "dp"), "kv", "tp", None),
        P(),
        P(),
        P("tp"),
    )
    out_specs = P(("grp", "dp"), "kv", "tp")
    return jax.shard_map(
        per_device, mesh=mesh, in_specs=in_specs, out_specs=out_specs, check_vma=False
    )
```

profile of v0, /device:TPU:0, one launch (start us, length us, event | category | flops | bytes accessed | tf_op | source)
XLA Modules:
  0.0 114.5 jit_solution(15482757723917872336)
XLA Ops:
  2.6 6.3 %all-to-all-start = ((s32[4,4,2]{1,2,0:T(2,128)}), s32[4,4,2]{1,2,0:T(2,128)S(1)}, u32[]{:S(2)}, u32[]{:S(2)}) async-start(s32[4,4,2]{1,2,0:T(2,128)} %copy.74), calls=%async_computation | async-start | bytes 8192 | tf_op jit(solution)/shard_map/all_to_all | solution.py:131
  9.6 1.3 %collective-permute-start.1 = (bf16[16,256]{1,0:T(8,128)(2,1)S(1)}, bf16[16,256]{1,0:T(8,128)(2,1)S(1)}, u32[]{:S(2)}, u32[]{:S(2)}) collective-permute-start(bf16[16,256]{1,0:T(8,128)(2,1)S(1)} %slice_bitcast_fusion.1), channel_id=1, source_target_pairs={{2,0},{4,2},{6,4},{3,1},{5,3},{7,5},{10,8},{12,10},{14,12},{11,9},... | collective-permute-start | bytes 24584 | tf_op jit(solution)/shard_map/ppermute | solution.py:23
  11.6 1.3 %collective-permute-start = (bf16[16,256]{1,0:T(8,128)(2,1)S(1)}, bf16[16,256]{1,0:T(8,128)(2,1)S(1)}, u32[]{:S(2)}, u32[]{:S(2)}) collective-permute-start(bf16[16,256]{1,0:T(8,128)(2,1)S(1)} %slice_bitcast_fusion.4), channel_id=1, source_target_pairs={{2,0},{4,2},{6,4},{3,1},{5,3},{7,5},{10,8},{12,10},{14,12},{11,9},... | collective-permute-start | bytes 24584 | tf_op jit(solution)/shard_map/ppermute | solution.py:23
  13.7 1.0 copy.73
  14.8 1.1 reshape_squeeze.9
  15.8 1.1 slice.65
  16.9 1.1 slice.72
  18.1 1.5 %gather_fusion.1 = s32[128]{0:T(128)S(1)} fusion(s32[4,16]{1,0:T(4,128)S(1)} %convert_subtract_fusion, s32[128]{0:T(128)S(1)} %reshape.454), kind=kCustom, calls=%fused_computation.1 | custom fusion | bytes 2048 | tf_op jit(solution)/shard_map/gather | solution.py:146
  26.7 1.1 reshape.513
  27.8 7.4 %all-to-all-start.2 = ((bf16[4,2,16384]{2,1,0:T(2,128)(2,1)}), bf16[4,2,16384]{2,1,0:T(2,128)(2,1)S(1)}, u32[]{:S(2)}, u32[]{:S(2)}) async-start(bf16[4,2,16384]{2,1,0:T(2,128)(2,1)} %reshape.513), calls=%async_computation.2 | async-start | bytes 524288 | tf_op jit(solution)/shard_map/all_to_all | solution.py:137
  35.9 1.1 reshape.511
  37.6 13.7 %all_gather.7 = bf16[64,4,64]{2,1,0:T(4,128)(2,1)S(1)} all-gather(bf16[16,4,64]{2,1,0:T(4,128)(2,1)S(1)} %fusion.39), channel_id=1, replica_groups=mesh['grp'=2,'dp'=2,'kv'=4,'tp'=2] {'kv'}, dimensions={0}, use_global_device_ids=true | all-gather | bytes 40960 | tf_op jit(solution)/shard_map/all_gather | solution.py:88
  51.6 13.3 %all_gather.6 = bf16[64,4,64]{2,0,1:T(8,128)(2,1)S(1)} all-gather(bf16[16,4,64]{2,0,1:T(8,128)(2,1)S(1)} %fusion.40), channel_id=1, replica_groups=mesh['grp'=2,'dp'=2,'kv'=4,'tp'=2] {'kv'}, dimensions={0}, use_global_device_ids=true | all-gather | bytes 40960 | tf_op jit(solution)/shard_map/all_gather | solution.py:87
  64.9 4.6 %all-to-all-start.1 = ((bf16[4,2,16384]{2,1,0:T(2,128)(2,1)}), bf16[4,2,16384]{2,1,0:T(2,128)(2,1)S(1)}, u32[]{:S(2)}, u32[]{:S(2)}) async-start(bf16[4,2,16384]{2,1,0:T(2,128)(2,1)} %reshape.511), calls=%async_computation.1 | async-start | bytes 524288 | tf_op jit(solution)/shard_map/all_to_all | solution.py:136
  69.5 5.2 %while.24 = (s32[]{:T(128)}, f32[4,4,256]{2,1,0:T(4,128)S(1)}, f32[4,4,256,64]{2,3,1,0:T(8,128)}, bf16[4,4,256,64]{2,3,1,0:T(8,128)(2,1)S(1)}, bf16[4,64,64]{2,1...) while((s32[]{:T(128)}, f32[4,4,256]{2,1,0:T(4,128)S(1)}, ...), condition=%wide.region_3.4_spmd.clone, body=%wide.region_0.3_spmd.clone.sunk | while | flops 17454080 | bytes 1326441 | solution.py:115
  75.1 1.2 %all-to-all-done.1 = bf16[4,2,16384]{2,1,0:T(2,128)(2,1)S(1)} async-done(((bf16[4,2,16384]{2,1,0:T(2,128)(2,1)}), bf16[4,2,16384]{2,1,0:T(2,128)(2,1)S(1)}, u32[]{:S(2)}, u32[]{:S(2)}) %all-to-all-start.1) | async-done | bytes 262176 | tf_op jit(solution)/shard_map/all_to_all | solution.py:136
  77.0 2.3 %gather_fusion.2 = bf16[128,64,64]{2,1,0:T(8,128)(2,1)} fusion(bf16[4,12,64,64]{3,2,1,0:T(8,128)(2,1)S(1)} %pad_maximum_fusion, s32[128]{0:T(128)S(1)} %reshape.460), kind=kCustom, calls=%fused_computation.2 | custom fusion | bytes 2098176 | tf_op jit(solution)/shard_map/gather | solution.py:147
  79.3 1.1 gather_fusion.4
  80.5 28.3 %while.23 = (s32[]{:T(128)}, f32[2,4,4,128,64]{3,4,2,1,0:T(8,128)}, s32[2,4,16]{2,1,0:T(4,128)S(1)}, s32[2]{0:T(128)S(1)}, s32[]{:T(128)}, /*index=5*/bf16[2,4,1...) while((s32[]{:T(128)}, f32[2,4,4,128,64]{3,4,2,1,0:T(8,128)}, ...), condition=%wide.region_10.11_spmd, body=%wide.region_7.10_spmd.sunk | while | flops 562172224 | bytes 65482908 | solution.py:177
  83.3 1.4 %compare_and_fusion.5 = pred[4,128,1024]{1,2,0:T(8,128)(4,1)S(1)} fusion(s32[128]{0:T(128)S(1)} %iota_add_fusion.5, s32[4,1024]{1,0:T(4,128)S(1)} %broadcast_add_fusion.2, pred[4,1024]{1,0:T(4,128)(4,1)S(1)} %and.110), kind=kLoop, calls=%fused_computation.15.clone.1 | loop fusion | flops 1048576 | bytes 545280 | tf_op jit(solution)/shard_map/while/body/eval_jaxpr/and | solution.py:163
  84.8 2.5 %select_reduce_fusion.5 = (f32[4,4,128]{2,1,0:T(4,128)S(1)}, f32[4,4,128,16,64]{2,4,1,3,0:T(8,128)S(1)}) fusion(pred[4,128,16,64]{1,3,2,0:T(8,128)(4,1)S(1)} %compare_and_fusion.4, bf16[2,128,4,4,64]{1,4,3,2,0:T(8,128)(2,1)} %get-tuple-element.346, s32[]{:T(128)S(6)} %copy.143, bf16[2,4,16,64,64]{4,3,2,1,0:T(8,128)(2,1)} %get-tuple-element.345), kind=kOutput, calls=%fused_computation.13.clone.1 | convolution fusion | flops 274724864 | bytes 10232832 | tf_op jit(solution)/shard_map/while/body/eval_jaxpr/tghd,gnkd->ghtnk/dot_general | solution.py:154
  87.3 2.1 %select_reduce_fusion.6 = f32[4,4,128]{2,1,0:T(4,128)S(1)} fusion(f32[4,4,128,16,64]{2,4,1,3,0:T(8,128)S(1)} %get-tuple-element.306, f32[4,4,128]{2,1,0:T(4,128)S(1)} %get-tuple-element.307, pred[4,128,16,64]{1,3,2,0:T(8,128)(4,1)S(1)} %compare_and_fusion.4), kind=kLoop, calls=%fused_computation.11.clone.1 | loop fusion | flops 8386560 | bytes 8929280 | tf_op jit(solution)/shard_map/while/body/eval_jaxpr/reduce_sum | solution.py:167
  90.3 2.4 %fusion.68 = bf16[4,4,128,1024]{2,3,1,0:T(8,128)(2,1)S(1)} fusion(f32[4,4,128,16,64]{2,4,3,1,0:T(8,128)S(1)} %copy.137, f32[4,4,128]{2,1,0:T(4,128)S(1)} %get-tuple-element.307, pred[4,128,1024]{1,2,0:T(8,128)(4,1)S(1)} %compare_and_fusion.5), kind=kLoop, calls=%fused_computation.10.clone.1 | loop fusion | flops 8388608 | bytes 13115392 | tf_op jit(solution)/shard_map/while/body/eval_jaxpr/convert_element_type | solution.py:171
  93.6 1.0 copy-done.1
  97.4 1.4 %compare_and_fusion.5 = pred[4,128,1024]{1,2,0:T(8,128)(4,1)S(1)} fusion(s32[128]{0:T(128)S(1)} %iota_add_fusion.5, s32[4,1024]{1,0:T(4,128)S(1)} %broadcast_add_fusion.2, pred[4,1024]{1,0:T(4,128)(4,1)S(1)} %and.110), kind=kLoop, calls=%fused_computation.15.clone.1 | loop fusion | flops 1048576 | bytes 545280 | tf_op jit(solution)/shard_map/while/body/eval_jaxpr/and | solution.py:163
  98.9 2.5 %select_reduce_fusion.5 = (f32[4,4,128]{2,1,0:T(4,128)S(1)}, f32[4,4,128,16,64]{2,4,1,3,0:T(8,128)S(1)}) fusion(pred[4,128,16,64]{1,3,2,0:T(8,128)(4,1)S(1)} %compare_and_fusion.4, bf16[2,128,4,4,64]{1,4,3,2,0:T(8,128)(2,1)} %get-tuple-element.346, s32[]{:T(128)S(6)} %copy.143, bf16[2,4,16,64,64]{4,3,2,1,0:T(8,128)(2,1)} %get-tuple-element.345), kind=kOutput, calls=%fused_computation.13.clone.1 | convolution fusion | flops 274724864 | bytes 10232832 | tf_op jit(solution)/shard_map/while/body/eval_jaxpr/tghd,gnkd->ghtnk/dot_general | solution.py:154
  101.4 2.1 %select_reduce_fusion.6 = f32[4,4,128]{2,1,0:T(4,128)S(1)} fusion(f32[4,4,128,16,64]{2,4,1,3,0:T(8,128)S(1)} %get-tuple-element.306, f32[4,4,128]{2,1,0:T(4,128)S(1)} %get-tuple-element.307, pred[4,128,16,64]{1,3,2,0:T(8,128)(4,1)S(1)} %compare_and_fusion.4), kind=kLoop, calls=%fused_computation.11.clone.1 | loop fusion | flops 8386560 | bytes 8929280 | tf_op jit(solution)/shard_map/while/body/eval_jaxpr/reduce_sum | solution.py:167
  104.4 2.4 %fusion.68 = bf16[4,4,128,1024]{2,3,1,0:T(8,128)(2,1)S(1)} fusion(f32[4,4,128,16,64]{2,4,3,1,0:T(8,128)S(1)} %copy.137, f32[4,4,128]{2,1,0:T(4,128)S(1)} %get-tuple-element.307, pred[4,128,1024]{1,2,0:T(8,128)(4,1)S(1)} %compare_and_fusion.5), kind=kLoop, calls=%fused_computation.10.clone.1 | loop fusion | flops 8388608 | bytes 13115392 | tf_op jit(solution)/shard_map/while/body/eval_jaxpr/convert_element_type | solution.py:171
  107.7 1.0 copy-done.1
  108.7 1.6 %fusion.33 = (f32[256,4,4]{0,2,1:T(4,128)S(1)}, f32[4,4,256,64]{2,3,1,0:T(8,128)S(1)}) fusion(f32[256,4,4]{0,2,1:T(4,128)S(1)} %mul.290, f32[256,4,4]{0,2,1:T(4,128)S(1)} %mul.287, f32[4,4,256,64]{2,3,1,0:T(8,128)S(1)} %copy-done.4, f32[4,4,256]{2,1,0:T(4,128)S(1)} %broadcast_maximum_fusion.1, f32[2,4,4,128,64]{3,4,2,1,0:T(8,128)} %get-tuple-element.87), kind=kLoop, calls=%fused_computation.57 | loop fusion | flops 1568768 | bytes 3211264 | tf_op jit(solution)/shard_map/reduce_sum | solution.py:184
  110.3 2.0 %copy.86 = f32[2,128,4,4,64]{1,0,4,3,2:T(2,128)S(1)} copy(f32[2,128,4,4,64]{1,4,3,2,0:T(8,128)} %bitcast.233) | data formatting | bytes 2097152 | tf_op jit(solution)/shard_map/transpose | solution.py:180
  113.5 1.0 copy.88
  (152 shorter events, 28.4 us)
Async XLA Ops:
  0.0 23.6 %copy-start.5 = (bf16[1,256,1024]{2,1,0:T(8,128)(2,1)S(1)}, bf16[1,256,1024]{2,1,0:T(8,128)(2,1)}, u32[]{:S(2)}) copy-start(bf16[1,256,1024]{2,1,0:T(8,128)(2,1)} %param.12) | copy-start | bytes 1572868
  2.6 23.2 %all-to-all-start = ((s32[4,4,2]{1,2,0:T(2,128)}), s32[4,4,2]{1,2,0:T(2,128)S(1)}, u32[]{:S(2)}, u32[]{:S(2)}) async-start(s32[4,4,2]{1,2,0:T(2,128)} %copy.74), calls=%async_computation | async-start | bytes 8192 | tf_op jit(solution)/shard_map/all_to_all | solution.py:131
  9.6 27.4 %collective-permute-start.1 = (bf16[16,256]{1,0:T(8,128)(2,1)S(1)}, bf16[16,256]{1,0:T(8,128)(2,1)S(1)}, u32[]{:S(2)}, u32[]{:S(2)}) collective-permute-start(bf16[16,256]{1,0:T(8,128)(2,1)S(1)} %slice_bitcast_fusion.1), channel_id=1, source_target_pairs={{2,0},{4,2},{6,4},{3,1},{5,3},{7,5},{10,8},{12,10},{14,12},{11,9},... | collective-permute-start | bytes 24584 | tf_op jit(solution)/shard_map/ppermute | solution.py:23
  11.6 25.8 %collective-permute-start = (bf16[16,256]{1,0:T(8,128)(2,1)S(1)}, bf16[16,256]{1,0:T(8,128)(2,1)S(1)}, u32[]{:S(2)}, u32[]{:S(2)}) collective-permute-start(bf16[16,256]{1,0:T(8,128)(2,1)S(1)} %slice_bitcast_fusion.4), channel_id=1, source_target_pairs={{2,0},{4,2},{6,4},{3,1},{5,3},{7,5},{10,8},{12,10},{14,12},{11,9},... | collective-permute-start | bytes 24584 | tf_op jit(solution)/shard_map/ppermute | solution.py:23
  19.6 17.4 %copy-start.2 = (bf16[1,256,256]{2,1,0:T(8,128)(2,1)S(1)}, bf16[1,256,256]{2,1,0:T(8,128)(2,1)}, u32[]{:S(2)}) copy-start(bf16[1,256,256]{2,1,0:T(8,128)(2,1)} %param.14) | copy-start | bytes 393220
  22.8 14.6 %copy-start.3 = (bf16[1,256,256]{2,1,0:T(8,128)(2,1)S(1)}, bf16[1,256,256]{2,1,0:T(8,128)(2,1)}, u32[]{:S(2)}) copy-start(bf16[1,256,256]{2,1,0:T(8,128)(2,1)} %param.13) | copy-start | bytes 393220
  27.8 37.1 %all-to-all-start.2 = ((bf16[4,2,16384]{2,1,0:T(2,128)(2,1)}), bf16[4,2,16384]{2,1,0:T(2,128)(2,1)S(1)}, u32[]{:S(2)}, u32[]{:S(2)}) async-start(bf16[4,2,16384]{2,1,0:T(2,128)(2,1)} %reshape.513), calls=%async_computation.2 | async-start | bytes 524288 | tf_op jit(solution)/shard_map/all_to_all | solution.py:137
  64.9 11.4 %all-to-all-start.1 = ((bf16[4,2,16384]{2,1,0:T(2,128)(2,1)}), bf16[4,2,16384]{2,1,0:T(2,128)(2,1)S(1)}, u32[]{:S(2)}, u32[]{:S(2)}) async-start(bf16[4,2,16384]{2,1,0:T(2,128)(2,1)} %reshape.511), calls=%async_computation.1 | async-start | bytes 524288 | tf_op jit(solution)/shard_map/all_to_all | solution.py:136
  74.7 5.7 %copy-start.6 = (s32[1,2,4,16]{3,2,1,0:T(4,128)S(1)}, s32[1,2,4,16]{3,2,1,0:T(4,128)}, u32[]{:S(2)}) copy-start(s32[1,2,4,16]{3,2,1,0:T(4,128)} %param.16) | copy-start | bytes 1540
  80.4 28.3 %copy-start.4 = (f32[4,4,256,64]{2,3,1,0:T(8,128)S(1)}, f32[4,4,256,64]{2,3,1,0:T(8,128)}, u32[]{:S(2)}) copy-start(f32[4,4,256,64]{2,3,1,0:T(8,128)} %get-tuple-element.85) | copy-start | bytes 3145732
  80.4 32.8 %copy-start.7 = (f32[1024]{0:T(1024)S(1)}, f32[1024]{0:T(1024)}, u32[]{:S(2)}) copy-start(f32[1024]{0:T(1024)} %param.19) | copy-start | bytes 12292
  90.3 2.4 %copy-start = (f32[2,4,4,128,64]{3,4,2,1,0:T(8,128)S(1)}, f32[2,4,4,128,64]{3,4,2,1,0:T(8,128)}, u32[]{:S(2)}) copy-start(f32[2,4,4,128,64]{3,4,2,1,0:T(8,128)} %get-tuple-element.331) | copy-start | bytes 3145732 | tf_op jit(solution)/shard_map/while
  93.6 1.0 copy-start.1
  104.4 2.4 %copy-start = (f32[2,4,4,128,64]{3,4,2,1,0:T(8,128)S(1)}, f32[2,4,4,128,64]{3,4,2,1,0:T(8,128)}, u32[]{:S(2)}) copy-start(f32[2,4,4,128,64]{3,4,2,1,0:T(8,128)} %get-tuple-element.331) | copy-start | bytes 3145732 | tf_op jit(solution)/shard_map/while
  107.7 1.0 copy-start.1
where the time goes:
time: 115 us; the launch traced here: 114 us
  local copies, waits for them, and re-layouts  29.9 us (26%)
  blocking collectives  27 us (23%)
  other arithmetic  22.1 us (19%)
  starting transfers between devices  21 us (18%)
  matrix products  11.2 us (10%)
  loops' own time  1.71 us (1%)
  waiting for transfers between devices  1.22 us (1%)
    all_gather x1, blocking collectives, per_device(): part_values = lax.all_gather(value_summary, 'kv', axis=0, tiled=True)  13.7 us
    all_gather x1, blocking collectives, per_device(): part_keys = lax.all_gather(key_summary, 'kv', axis=0, tiled=True)  13.3 us
    all_to_all x1, starting transfers between devices, per_device(): lax.all_to_all(served[1], 'kv', split_axis=0, concat_axis=0, tiled=True)  7.44 us
    all_to_all x1, starting transfers between devices, per_device(): lax.all_to_all(asked_ids, 'kv', split_axis=0, concat_axis=0, tiled=True)  6.35 us
    unnamed x21, local copies, waits for them, and re-layouts  5.66 us
    dot_general x2, matrix products, attend(): jnp.einsum('tghd,gnkd->ghtnk', query_part, keys_part, preferred_element_t...  5.03 us
    convert_element_type x2, other arithmetic, attend(): weight.astype(jnp.bfloat16)  4.81 us
    and x4, other arithmetic, attend(): live[:, None, :] & (key_place[:, None, :] <= place_q[None, :, None])  4.65 us
  transfers between devices with their start and end apart: 5, of which 1 were waited for; matrix products, arithmetic and copies ran while one was open for 21% of the time, Pallas kernels for 0%

commit v1 on v0

v1 whole, which is shorter than its diff:
```python
import functools

import jax
import jax.numpy as jnp
from jax import lax
from jax.experimental import pallas as pl
from jax.experimental.pallas import tpu as pltpu
from jax.sharding import PartitionSpec as P

DH = 64
CMP_STRIDE = 16
CMP_BLOCK = 32
SLC = 64
QB = 128
MOST = 2
THETA = 500000.0
EPS = 1e-06
NEG = -1e30
LOG2E = 1.4426950408889634
MESH = pl.DeviceIdType.MESH


def rope_table(start, length):
    half = DH // 2
    lane = jnp.arange(2 * DH)
    freq = jnp.power(jnp.float32(THETA), -(2.0 * (lane % half).astype(jnp.float32)) / DH)
    angle = (start + jnp.arange(length)).astype(jnp.float32)[:, None] * freq[None, :]
    sign = jnp.where(lane % DH < half, -1.0, 1.0).astype(jnp.float32)
    return jnp.cos(angle), jnp.sin(angle) * sign[None, :]


def turn(x, cosine, sine):
    half = DH // 2
    lane = lax.broadcasted_iota(jnp.int32, x.shape, 1)
    partner = jnp.where(lane % DH < half, pltpu.roll(x, 2 * DH - half, 1), pltpu.roll(x, half, 1))
    return (x * cosine + partner * sine).astype(jnp.bfloat16)


def kernel(
    n, q_ref, k_ref, v_ref, gate_ref, list_ref, pk_ref, pv_ref, gain_ref, cos_ref, sin_ref,
    out_ref,
    qt, kt, vtl, kk, kkr, vtr, skk, svt, req, reqbuf, flag, own_bias, far_bias,
    sumbuf, edge, sendk, sendv, recvk, recvv, bias,
    top, total, acc, stot, sacc,
    req_send, req_recv, sum_send, sum_recv, edge_send, edge_recv,
    k_send, k_recv, v_send, v_recv,
):
    me = lax.axis_index("kv")
    length = q_ref.shape[1]
    heads = q_ref.shape[2] // DH
    groups = k_ref.shape[2] // DH
    per_group = heads // groups
    pairs = per_group // 2
    slabs = groups // 2
    qblocks = length // QB
    per = length // SLC
    count = length // CMP_STRIDE
    scale = DH ** (-0.5) * LOG2E
    f32 = jnp.float32

    barrier = pltpu.get_barrier_semaphore()
    for d in range(1, n):
        pl.semaphore_signal(
            barrier, inc=1, device_id={"kv": lax.rem(me + d, n)}, device_id_type=MESH
        )

    lanes = req.shape[1]
    rows = qblocks * groups

    def column(x, at):
        spot = lax.broadcasted_iota(jnp.int32, x.shape, 1) == at
        picked = jnp.sum(jnp.where(spot, x.astype(f32), 0.0), 1, keepdims=True)
        return jnp.broadcast_to(picked, (x.shape[0], QB))

    lists = jnp.concatenate([list_ref[0, b] for b in range(qblocks)], 0)
    lane = lax.broadcasted_iota(jnp.int32, (rows, lanes), 1)
    member = jnp.zeros((rows, lanes), jnp.int32)
    for i in range(lists.shape[1]):
        member = jnp.where(lists[:, i : i + 1] == lane, 1, member)
    union = member[:groups]
    for b in range(1, qblocks):
        union = jnp.maximum(union, member[b * groups : (b + 1) * groups])
    union = jnp.concatenate([union] * qblocks, 0)
    inner = lane % per
    rank = jnp.zeros_like(union)
    for d in range(1, per):
        rank = rank + jnp.where(inner >= d, pltpu.roll(union, d, 1), 0)

    def first_of(x):
        found = x
        for d in range(1, per):
            found = found + pltpu.roll(x, lanes - d, 1)
        return found

    for j in range(MOST):
        hit = (union == 1) & (rank == j)
        asked = first_of(jnp.where(hit, inner, 0))
        req[j * groups : (j + 1) * groups, :] = asked[:groups]
        flag[j * rows : (j + 1) * rows, :] = first_of(jnp.where(hit, member, 0))
    for i in range(per):
        own_bias[i] = jnp.where(column(member, me * per + i) > 0.5, 0.0, NEG)

    pl.semaphore_wait(barrier, n - 1)

    def remote(src, dst, send, recv, peer, origin):
        return pltpu.make_async_remote_copy(
            src_ref=src, dst_ref=dst, send_sem=send.at[peer], recv_sem=recv.at[origin],
            device_id={"kv": peer}, device_id_type=MESH,
        )

    def ask(peer, origin):
        return remote(req, reqbuf.at[origin], req_send, req_recv, peer, origin)

    def give_sum(peer, origin):
        return remote(sumbuf.at[origin], sumbuf.at[origin], sum_send, sum_recv, peer, origin)

    def give_edge(peer, origin):
        return remote(edge.at[origin], edge.at[origin], edge_send, edge_recv, peer, origin)

    def give_k(peer, origin):
        return remote(sendk.at[peer], recvk.at[origin], k_send, k_recv, peer, origin)

    def give_v(peer, origin):
        return remote(sendv.at[peer], recvv.at[origin], v_send, v_recv, peer, origin)

    @pl.loop(0, me)
    def _(d):
        ask(me - 1 - d, me).start()

    cosine = cos_ref[...]
    sine = sin_ref[...]
    low = lax.broadcasted_iota(jnp.int32, (length, 2 * DH), 1) < DH
    for p in range(slabs):
        cols = slice(p * 2 * DH, (p + 1) * 2 * DH)
        turned = turn(k_ref[0, :, cols].astype(f32), cosine, sine)
        kt[:, cols] = turned
    row = lax.broadcasted_iota(jnp.int32, (count, 2 * DH), 0)
    for w, (src, pool_ref) in enumerate(((k_ref, pk_ref), (v_ref, pv_ref))):
        pool = pool_ref[...]
        pool = jnp.concatenate([pool, pool], 1)
        for p in range(slabs):
            cols = slice(p * 2 * DH, (p + 1) * 2 * DH)
            x = src[0, :, cols].astype(f32).reshape(count, CMP_STRIDE, 2 * DH)
            lower = jnp.sum(x * pool[None, :CMP_STRIDE], 1)
            upper = jnp.sum(x * pool[None, CMP_STRIDE:], 1)
            following = jnp.where(row == count - 1, 0.0, pltpu.roll(upper, count - 1, 0))
            sumbuf[me, w, :, cols] = (lower + following).astype(jnp.bfloat16)
            edge[me, 2 * w : 2 * w + 1, cols] = lower[count - 1 :]
            edge[me, 2 * w + 1 : 2 * w + 2, cols] = upper[:1]

    @pl.loop(me + 1, n)
    def _(r):
        give_sum(r, me).start()
        give_edge(r, me).start()

    low_slc = lax.broadcasted_iota(jnp.int32, (SLC, 2 * DH), 1) < DH

    @pl.loop(me + 1, n)
    def _(r):
        ask(me, r).wait_recv()
        ids = column(reqbuf[r], me * per)
        for j in range(MOST):
            place = slice(j * SLC, (j + 1) * SLC)
            for p in range(slabs):
                cols = slice(p * 2 * DH, (p + 1) * 2 * DH)
                at = j * groups + 2 * p
                pick = jnp.where(low_slc, ids[at : at + 1], ids[at + 1 : at + 2])
                k_block = kt[:SLC, cols].astype(f32)
                v_block = v_ref[0, :SLC, cols].astype(f32)
                for i in range(1, per):
                    span = slice(i * SLC, (i + 1) * SLC)
                    match = pick > i - 0.5
                    k_block = jnp.where(match, kt[span, cols].astype(f32), k_block)
                    v_block = jnp.where(match, v_ref[0, span, cols].astype(f32), v_block)
                sendk[r, place, cols] = k_block.astype(jnp.bfloat16)
                sendv[r, place, cols] = v_block.astype(jnp.bfloat16)
        give_k(r, me).start()
        give_v(r, me).start()

    @pl.loop(0, heads // 2)
    def _(p):
        cols = pl.ds(pl.multiple_of(p * 2 * DH, 2 * DH), 2 * DH)
        qt[p] = turn(q_ref[0, :, cols].astype(f32), cosine, sine)

    def spread(slab, g, dst):
        keep = lax.broadcasted_iota(jnp.int32, slab.shape, 1) < DH
        wide = slab.astype(f32)
        swapped = pltpu.roll(wide, DH, 1)
        first, second = (wide, swapped) if g % 2 == 0 else (swapped, wide)
        dst[g, 0] = jnp.where(keep, first, 0.0).astype(jnp.bfloat16)
        dst[g, 1] = jnp.where(keep, 0.0, second).astype(jnp.bfloat16)

    def transposed(slab):
        return slab.astype(f32).T.astype(jnp.bfloat16)

    def score(keys, queries):
        return lax.dot_general(
            keys, queries, (((1,), (1,)), ((), ())), preferred_element_type=f32
        )

    for g in range(groups):
        spread(kt[:, (g // 2) * 2 * DH : (g // 2 + 1) * 2 * DH], g, kk)
    for p in range(slabs):
        flip = transposed(v_ref[0, :, p * 2 * DH : (p + 1) * 2 * DH])
        vtl[2 * p] = flip[:DH]
        vtl[2 * p + 1] = flip[DH:]
    key_at = lax.broadcasted_iota(jnp.int32, (SLC, QB), 0)
    token_at = lax.broadcasted_iota(jnp.int32, (SLC, QB), 1)

    @pl.loop(0, groups)
    def _(g):
        for b in range(qblocks):
            for i in range(per):
                value = own_bias[i, pl.ds(b * groups + g, 1), :]
                tile = jnp.where(key_at + i * SLC <= token_at + b * QB, value, NEG)
                bias[i * SLC : (i + 1) * SLC, b * QB : (b + 1) * QB] = tile
        for pair in range(pairs):
            queries = qt[g * pairs + pair]
            for e in range(2):
                h = g * per_group + 2 * pair + e
                s = score(kk[g, e], queries) * scale + bias[...]
                m = jnp.max(s, 0, keepdims=True)
                w = jnp.exp2(s - m)
                top[h] = m
                total[h] = jnp.sum(w, 0, keepdims=True)
                acc[h] = jnp.dot(vtl[g], w.astype(jnp.bfloat16), preferred_element_type=f32)

    @pl.loop(0, me)
    def _(d):
        give_sum(me, me - 1 - d).wait_recv()
        give_edge(me, me - 1 - d).wait_recv()

    for s in range(n):
        for w in range(2):
            place = slice(s * count, (s + 1) * count)
            for p in range(slabs):
                cols = slice(p * 2 * DH, (p + 1) * 2 * DH)
                following = edge[min(s + 1, n - 1), 2 * w + 1 : 2 * w + 2, cols]
                last = edge[s, 2 * w : 2 * w + 1, cols] + following
                own = sumbuf[s, w, :, cols].astype(f32)
                joined = jnp.where((row == count - 1) & (s < me), last, own)
                joined = jnp.where(s <= me, joined, 0.0)
                if w == 0:
                    for o in range(2):
                        lanes_low = lax.broadcasted_iota(jnp.int32, joined.shape, 1) < DH
                        swapped = pltpu.roll(joined, DH, 1)
                        first, second = (joined, swapped) if o == 0 else (swapped, joined)
                        skk[2 * p + o, 0, place] = jnp.where(lanes_low, first, 0.0).astype(
                            jnp.bfloat16
                        )
                        skk[2 * p + o, 1, place] = jnp.where(lanes_low, 0.0, second).astype(
                            jnp.bfloat16
                        )
                else:
                    svt[place, cols] = joined.astype(jnp.bfloat16)
    part_at = lax.broadcasted_iota(jnp.int32, (n * count, length), 0)
    time_at = lax.broadcasted_iota(jnp.int32, (n * count, length), 1) + me * length
    seen = part_at * CMP_STRIDE + CMP_BLOCK - 1 <= time_at
    sbias = jnp.where(seen, 0.0, NEG)
    flips = [transposed(svt[:, p * 2 * DH : (p + 1) * 2 * DH]) for p in range(slabs)]
    for g in range(groups):
        vt = flips[g // 2][(g % 2) * DH : (g % 2 + 1) * DH]
        for pair in range(pairs):
            queries = q_ref[0, :, (g * pairs + pair) * 2 * DH : (g * pairs + pair + 1) * 2 * DH]
            for e in range(2):
                h = g * per_group + 2 * pair + e
                s = score(skk[g, e], queries) * scale + sbias
                m = jnp.maximum(jnp.max(s, 0, keepdims=True), 0.1 * NEG)
                w = jnp.exp2(s - m)
                stot[h] = jnp.sum(w, 0, keepdims=True)
                sacc[h] = jnp.dot(vt, w.astype(jnp.bfloat16), preferred_element_type=f32)

    @pl.loop(0, me)
    def _(d):
        s = me - 1 - d
        give_k(me, s).wait_recv()
        give_v(me, s).wait_recv()
        far_bias[...] = jnp.where(column(flag[...], s * per) > 0.5, 0.0, NEG)
        for g in range(groups):
            spread(recvk[s, :, (g // 2) * 2 * DH : (g // 2 + 1) * 2 * DH], g, kkr)
        for p in range(slabs):
            flip = transposed(recvv[s, :, p * 2 * DH : (p + 1) * 2 * DH])
            vtr[2 * p] = flip[:DH]
            vtr[2 * p + 1] = flip[DH:]

        @pl.loop(0, groups)
        def _(g):
            rowed = [
                jnp.concatenate(
                    [
                        far_bias[pl.ds((j * qblocks + b) * groups + g, 1), :]
                        for b in range(qblocks)
                    ],
                    1,
                )
                for j in range(MOST)
            ]
            for pair in range(pairs):
                queries = qt[g * pairs + pair]
                for e in range(2):
                    h = g * per_group + 2 * pair + e
                    raw = score(kkr[g, e], queries) * scale
                    sc = jnp.concatenate(
                        [raw[j * SLC : (j + 1) * SLC] + rowed[j] for j in range(MOST)], 0
                    )
                    old = top[h]
                    m = jnp.maximum(jnp.max(sc, 0, keepdims=True), old)
                    w = jnp.exp2(sc - m)
                    shrink = jnp.exp2(old - m)
                    top[h] = m
                    total[h] = total[h] * shrink + jnp.sum(w, 0, keepdims=True)
                    acc[h] = acc[h] * shrink + jnp.dot(
                        vtr[g], w.astype(jnp.bfloat16), preferred_element_type=f32
                    )

    for pair in range(heads // 2):
        both = []
        for e in range(2):
            h = 2 * pair + e
            mixed = sacc[h] * (gate_ref[0, h : h + 1] / jnp.maximum(stot[h], 1.0)) + acc[h] * (
                gate_ref[1, h : h + 1] / total[h]
            )
            mean = jnp.sum(mixed * mixed, 0, keepdims=True) * (1.0 / DH)
            both.append(mixed * lax.rsqrt(mean + EPS))
        cols = slice(pair * 2 * DH, (pair + 1) * 2 * DH)
        flat = jnp.concatenate(both, 0).T
        out_ref[0, :, cols] = (flat * gain_ref[:, cols]).astype(jnp.bfloat16)

    @pl.loop(0, me)
    def _(d):
        ask(me - 1 - d, me).wait_send()

    @pl.loop(me + 1, n)
    def _(r):
        give_sum(r, me).wait_send()
        give_edge(r, me).wait_send()
        give_k(r, me).wait_send()
        give_v(r, me).wait_send()


def per_device(queries, keys, values, gate_logits, chosen, pool_k, pool_v, out_gain):
    n = lax.axis_size("kv")
    length = queries.shape[1]
    groups = keys.shape[2] // DH
    heads = queries.shape[2] // DH
    qblocks = length // QB
    count = length // CMP_STRIDE
    total = n * (length // SLC)
    lanes = -(-total // 128) * 128
    rows = qblocks * groups
    width = groups * DH
    cosine, sine = rope_table(lax.axis_index("kv") * length, length)
    gates = jax.nn.sigmoid(gate_logits[0]).transpose(0, 2, 1)
    bf16, f32, i32 = jnp.bfloat16, jnp.float32, jnp.int32
    vm, dma = pltpu.VMEM, pltpu.SemaphoreType.DMA
    scratch = [
        vm((heads // 2, length, 2 * DH), bf16),
        vm((length, width), bf16),
        vm((groups, DH, length), bf16),
        vm((groups, 2, length, 2 * DH), bf16),
        vm((groups, 2, MOST * SLC, 2 * DH), bf16),
        vm((groups, DH, MOST * SLC), bf16),
        vm((groups, 2, n * count, 2 * DH), bf16),
        vm((n * count, width), bf16),
        vm((MOST * groups, lanes), i32),
        vm((n, MOST * groups, lanes), i32),
        vm((MOST * rows, lanes), i32),
        vm((length // SLC, rows, QB), f32),
        vm((MOST * rows, QB), f32),
        vm((n, 2, count, width), bf16),
        vm((n, 8, width), f32),
        vm((n, MOST * SLC, width), bf16),
        vm((n, MOST * SLC, width), bf16),
        vm((n, MOST * SLC, width), bf16),
        vm((n, MOST * SLC, width), bf16),
        vm((length, length), f32),
        vm((heads, 1, length), f32),
        vm((heads, 1, length), f32),
        vm((heads, DH, length), f32),
        vm((heads, 1, length), f32),
        vm((heads, DH, length), f32),
        dma((n,)), dma((n,)), dma((n,)), dma((n,)), dma((n,)), dma((n,)),
        dma((n,)), dma((n,)), dma((n,)), dma((n,)),
    ]
    return pl.pallas_call(
        functools.partial(kernel, n),
        out_shape=jax.ShapeDtypeStruct(queries.shape, bf16),
        in_specs=[pl.BlockSpec(memory_space=pltpu.VMEM)] * 10,
        out_specs=pl.BlockSpec(memory_space=pltpu.VMEM),
        scratch_shapes=scratch,
        compiler_params=pltpu.CompilerParams(
            collective_id=0, has_side_effects=True, vmem_limit_bytes=48 << 20
        ),
    )(queries, keys, values, gates, chosen, pool_k, pool_v, out_gain[None], cosine, sine)


def solution(mesh):
    in_specs = (
        P(("grp", "dp"), "kv", "tp"),
        P(("grp", "dp"), "kv", "tp"),
        P(("grp", "dp"), "kv", "tp"),
        P(("grp", "dp"), None, "kv", "tp"),
        P(("grp", "dp"), "kv", "tp", None),
        P(),
        P(),
        P("tp"),
    )
    out_specs = P(("grp", "dp"), "kv", "tp")
    return jax.shard_map(
        per_device, mesh=mesh, in_specs=in_specs, out_specs=out_specs, check_vma=False
    )
```

time: 115 us -> 29.5 us (0.26)
  the two profiles are of different devices: /device:TPU:0 before, /device:TPU:24 now
where the time goes in v1:
time: 29.5 us; the launch traced here: 29.2 us
  Pallas kernels  25.5 us (86%)
  local copies, waits for them, and re-layouts  2.23 us (8%)
  other arithmetic  1.34 us (5%)
    pallas_call x1, Pallas kernels, per_device(): pl.pallas_call(functools.partial(kernel, n), out_shape=jax.ShapeDtypeStru...  25.5 us
    unnamed x15, local copies, waits for them, and re-layouts  2.23 us
    transpose x1, other arithmetic, per_device(): gates = jax.nn.sigmoid(gate_logits[0]).transpose(0, 2, 1)  0.79 us

profile of v1, /device:TPU:24, one launch (start us, length us, event | category | flops | bytes accessed | tf_op | source)
XLA Modules:
  0.0 29.2 jit_solution(5449256941560458672)
XLA Ops:
  0.0 0.0 copy-start.3
  0.0 0.0 copy-start.4
  0.0 0.0 copy-start.6
  0.1 0.8 %divide_bitcast_fusion.gate_ref = f32[2,16,256]{2,1,0:T(8,128)S(1)} fusion(f32[1,2,256,16]{2,3,1,0:T(8,128)} %param.11), kind=kLoop, calls=%fused_computation.3 | loop fusion | flops 24576 | bytes 65536 | tf_op jit(solution)/shard_map/transpose | solution.py:353
  0.8 0.0 copy-start.1
  0.9 0.0 copy-start.2
  0.9 0.0 copy-start.5
  0.9 0.5 %fusion = (f32[256,128]{1,0:T(8,128)S(1)}, f32[256,128]{1,0:T(8,128)S(1)}) fusion(f32[128]{0:T(128)S(1)} %get-tuple-element.7, f32[128]{0:T(128)S(1)} %get-tuple-element.8, f32[256]{0:T(256)S(1)} %add_convert_fusion), kind=kLoop, calls=%fused_computation.2 | loop fusion | flops 65536 | bytes 264192 | tf_op jit(solution)/shard_map/mul | solution.py:29
  1.4 0.0 copy-done.3
  1.4 0.0 copy-done.4
  1.4 0.0 copy-done.6
  1.5 0.3 %copy-done.1 = bf16[1,256,256]{2,1,0:T(8,128)(2,1)S(1)} copy-done((bf16[1,256,256]{2,1,0:T(8,128)(2,1)S(1)}, bf16[1,256,256]{2,1,0:T(8,128)(2,1)}, u32[]{:S(2)}) %copy-start.1) | copy-done | bytes 131096
  1.8 0.1 copy-done.2
  1.8 0.0 copy-done.5
  1.8 0.0 copy-start
  1.8 1.0 %copy-done = bf16[1,256,1024]{2,1,0:T(8,128)(2,1)S(1)} copy-done((bf16[1,256,1024]{2,1,0:T(8,128)(2,1)S(1)}, bf16[1,256,1024]{2,1,0:T(8,128)(2,1)}, u32[]{:S(2)}) %copy-start) | copy-done | bytes 524312
  2.9 25.5 %shard_map.82 = bf16[1,256,1024]{2,1,0:T(8,128)(2,1)S(1)} custom-call(bf16[1,256,1024]{2,1,0:T(8,128)(2,1)S(1)} %copy-done, bf16[1,256,256]{2,1,0:T(8,128)(2,1)S(1)} %copy-done.1, bf16[1,256,256]{2,1,0:T(8,128)(2,1)S(1)} %copy-done.2, f32[2,16,256]{2,1,0:T(8,128)S(1)} %divide_bitcast_fusion.gate_ref, s32[1,2,4,16]{3,2,1,0:T(4,128)S(1)} %copy-done.5, ...), custom_call_target="tpu_custom_call" | custom-call | tf_op jit(solution)/shard_map/pallas_call | solution.py:385
  28.4 0.8 %copy.10 = bf16[1,256,1024]{2,1,0:T(8,128)(2,1)} copy(bf16[1,256,1024]{2,1,0:T(8,128)(2,1)S(1)} %shard_map.82) | data formatting | bytes 1048576
  (2 shorter events, 0.0 us)
Async XLA Ops:
  0.0 1.4 %copy-start.3 = (f32[32,64]{1,0:T(8,128)S(1)}, f32[32,64]{1,0:T(8,128)}, u32[]{:S(2)}) copy-start(f32[32,64]{1,0:T(8,128)} %pk_ref.1) | copy-start | bytes 24580
  0.0 1.4 %copy-start.4 = (f32[32,64]{1,0:T(8,128)S(1)}, f32[32,64]{1,0:T(8,128)}, u32[]{:S(2)}) copy-start(f32[32,64]{1,0:T(8,128)} %pv_ref.1) | copy-start | bytes 24580
  0.0 1.4 %copy-start.6 = (f32[1024]{0:T(1024)S(1)}, f32[1024]{0:T(1024)}, u32[]{:S(2)}) copy-start(f32[1024]{0:T(1024)} %param.15) | copy-start | bytes 12292
  0.8 0.9 %copy-start.1 = (bf16[1,256,256]{2,1,0:T(8,128)(2,1)S(1)}, bf16[1,256,256]{2,1,0:T(8,128)(2,1)}, u32[]{:S(2)}) copy-start(bf16[1,256,256]{2,1,0:T(8,128)(2,1)} %k_ref.1) | copy-start | bytes 393220
  0.9 1.0 %copy-start.2 = (bf16[1,256,256]{2,1,0:T(8,128)(2,1)S(1)}, bf16[1,256,256]{2,1,0:T(8,128)(2,1)}, u32[]{:S(2)}) copy-start(bf16[1,256,256]{2,1,0:T(8,128)(2,1)} %v_ref.1) | copy-start | bytes 393220
  0.9 1.0 %copy-start.5 = (s32[1,2,4,16]{3,2,1,0:T(4,128)S(1)}, s32[1,2,4,16]{3,2,1,0:T(4,128)}, u32[]{:S(2)}) copy-start(s32[1,2,4,16]{3,2,1,0:T(4,128)} %list_ref.1) | copy-start | bytes 1540
  1.8 1.0 %copy-start = (bf16[1,256,1024]{2,1,0:T(8,128)(2,1)S(1)}, bf16[1,256,1024]{2,1,0:T(8,128)(2,1)}, u32[]{:S(2)}) copy-start(bf16[1,256,1024]{2,1,0:T(8,128)(2,1)} %q_ref.1) | copy-start | bytes 1572868

commit v2 on v1

--- a/solution.py
+++ b/solution.py
@@ -155,8 +155,11 @@
 
     low_slc = lax.broadcasted_iota(jnp.int32, (SLC, 2 * DH), 1) < DH
 
-    @pl.loop(me + 1, n)
-    def _(r):
+    odd = lax.rem(me, 2)
+
+    @pl.loop(0, n - 1 - me)
+    def _(d):
+        r = odd * (me + 1 + d) + (1 - odd) * (n - 1 - d)
         ask(me, r).wait_recv()
         ids = column(reqbuf[r], me * per)
         for j in range(MOST):
@@ -177,10 +180,8 @@
         give_k(r, me).start()
         give_v(r, me).start()
 
-    @pl.loop(0, heads // 2)
-    def _(p):
-        cols = pl.ds(pl.multiple_of(p * 2 * DH, 2 * DH), 2 * DH)
-        qt[p] = turn(q_ref[0, :, cols].astype(f32), cosine, sine)
+    for p in range(heads // 2):
+        qt[p] = turn(q_ref[0, :, p * 2 * DH : (p + 1) * 2 * DH].astype(f32), cosine, sine)
 
     def spread(slab, g, dst):
         keep = lax.broadcasted_iota(jnp.int32, slab.shape, 1) < DH
@@ -207,23 +208,31 @@
     key_at = lax.broadcasted_iota(jnp.int32, (SLC, QB), 0)
     token_at = lax.broadcasted_iota(jnp.int32, (SLC, QB), 1)
 
-    @pl.loop(0, groups)
+    @pl.loop(0, groups, unroll=2)
     def _(g):
         for b in range(qblocks):
             for i in range(per):
                 value = own_bias[i, pl.ds(b * groups + g, 1), :]
                 tile = jnp.where(key_at + i * SLC <= token_at + b * QB, value, NEG)
                 bias[i * SLC : (i + 1) * SLC, b * QB : (b + 1) * QB] = tile
-        for pair in range(pairs):
-            queries = qt[g * pairs + pair]
-            for e in range(2):
-                h = g * per_group + 2 * pair + e
-                s = score(kk[g, e], queries) * scale + bias[...]
-                m = jnp.max(s, 0, keepdims=True)
-                w = jnp.exp2(s - m)
-                top[h] = m
-                total[h] = jnp.sum(w, 0, keepdims=True)
-                acc[h] = jnp.dot(vtl[g], w.astype(jnp.bfloat16), preferred_element_type=f32)
+        both = kk[g].reshape(2 * length, 2 * DH)
+        allowed = bias[...]
+        raw = [score(both, qt[g * pairs + pair]) * scale for pair in range(pairs)]
+        parts = [
+            r[e * length : (e + 1) * length] + allowed for r in raw for e in range(2)
+        ]
+        tops = [jnp.max(x, 0, keepdims=True) for x in parts]
+        weights = [jnp.exp2(x - m) for x, m in zip(parts, tops)]
+        totals = [jnp.sum(w, 0, keepdims=True) for w in weights]
+        flat = vtl[g]
+        sums = [
+            jnp.dot(flat, w.astype(jnp.bfloat16), preferred_element_type=f32) for w in weights
+        ]
+        for o in range(per_group):
+            h = g * per_group + o
+            top[h] = tops[o]
+            total[h] = totals[o]
+            acc[h] = sums[o]
 
     @pl.loop(0, me)
     def _(d):
@@ -260,19 +269,26 @@
     flips = [transposed(svt[:, p * 2 * DH : (p + 1) * 2 * DH]) for p in range(slabs)]
     for g in range(groups):
         vt = flips[g // 2][(g % 2) * DH : (g % 2 + 1) * DH]
-        for pair in range(pairs):
-            queries = q_ref[0, :, (g * pairs + pair) * 2 * DH : (g * pairs + pair + 1) * 2 * DH]
-            for e in range(2):
-                h = g * per_group + 2 * pair + e
-                s = score(skk[g, e], queries) * scale + sbias
-                m = jnp.maximum(jnp.max(s, 0, keepdims=True), 0.1 * NEG)
-                w = jnp.exp2(s - m)
-                stot[h] = jnp.sum(w, 0, keepdims=True)
-                sacc[h] = jnp.dot(vt, w.astype(jnp.bfloat16), preferred_element_type=f32)
+        both = skk[g].reshape(2 * n * count, 2 * DH)
+        raw = [
+            score(both, q_ref[0, :, (g * pairs + pair) * 2 * DH : (g * pairs + pair + 1) * 2 * DH])
+            * scale
+            for pair in range(pairs)
+        ]
+        parts = [
+            r[e * n * count : (e + 1) * n * count] + sbias for r in raw for e in range(2)
+        ]
+        tops = [jnp.maximum(jnp.max(x, 0, keepdims=True), 0.1 * NEG) for x in parts]
+        weights = [jnp.exp2(x - m) for x, m in zip(parts, tops)]
+        totals = [jnp.sum(w, 0, keepdims=True) for w in weights]
+        sums = [jnp.dot(vt, w.astype(jnp.bfloat16), preferred_element_type=f32) for w in weights]
+        for o in range(per_group):
+            stot[g * per_group + o] = totals[o]
+            sacc[g * per_group + o] = sums[o]
 
     @pl.loop(0, me)
     def _(d):
-        s = me - 1 - d
+        s = lax.rem(me - 1 + d, me)
         give_k(me, s).wait_recv()
         give_v(me, s).wait_recv()
         far_bias[...] = jnp.where(column(flag[...], s * per) > 0.5, 0.0, NEG)
@@ -283,7 +299,7 @@
             vtr[2 * p] = flip[:DH]
             vtr[2 * p + 1] = flip[DH:]
 
-        @pl.loop(0, groups)
+        @pl.loop(0, groups, unroll=4)
         def _(g):
             rowed = [
                 jnp.concatenate(
@@ -295,30 +311,50 @@
                 )
                 for j in range(MOST)
             ]
-            for pair in range(pairs):
-                queries = qt[g * pairs + pair]
-                for e in range(2):
-                    h = g * per_group + 2 * pair + e
-                    raw = score(kkr[g, e], queries) * scale
-                    sc = jnp.concatenate(
-                        [raw[j * SLC : (j + 1) * SLC] + rowed[j] for j in range(MOST)], 0
-                    )
-                    old = top[h]
-                    m = jnp.maximum(jnp.max(sc, 0, keepdims=True), old)
-                    w = jnp.exp2(sc - m)
-                    shrink = jnp.exp2(old - m)
-                    top[h] = m
-                    total[h] = total[h] * shrink + jnp.sum(w, 0, keepdims=True)
-                    acc[h] = acc[h] * shrink + jnp.dot(
-                        vtr[g], w.astype(jnp.bfloat16), preferred_element_type=f32
-                    )
+            size = MOST * SLC
+            both = kkr[g].reshape(2 * size, 2 * DH)
+            base = g * per_group
+            old = [top[base + o] for o in range(per_group)]
+            old_total = [total[base + o] for o in range(per_group)]
+            old_acc = [acc[base + o] for o in range(per_group)]
+            raw = [score(both, qt[g * pairs + pair]) * scale for pair in range(pairs)]
+            parts = [
+                jnp.concatenate(
+                    [
+                        r[e * size + j * SLC : e * size + (j + 1) * SLC] + rowed[j]
+                        for j in range(MOST)
+                    ],
+                    0,
+                )
+                for r in raw
+                for e in range(2)
+            ]
+            tops = [jnp.maximum(jnp.max(x, 0, keepdims=True), m) for x, m in zip(parts, old)]
+            weights = [jnp.exp2(x - m) for x, m in zip(parts, tops)]
+            shrink = [jnp.exp2(a - m) for a, m in zip(old, tops)]
+            totals = [
+                t * c + jnp.sum(w, 0, keepdims=True)
+                for t, c, w in zip(old_total, shrink, weights)
+            ]
+            flat = vtr[g]
+            sums = [
+                a * c + jnp.dot(flat, w.astype(jnp.bfloat16), preferred_element_type=f32)
+                for a, c, w in zip(old_acc, shrink, weights)
+            ]
+            for o in range(per_group):
+                top[base + o] = tops[o]
+                total[base + o] = totals[o]
+                acc[base + o] = sums[o]
 
     for pair in range(heads // 2):
         both = []
         for e in range(2):
             h = 2 * pair + e
-            mixed = sacc[h] * (gate_ref[0, h : h + 1] / jnp.maximum(stot[h], 1.0)) + acc[h] * (
-                gate_ref[1, h : h + 1] / total[h]
+            first, second = (
+                1.0 / (1.0 + jnp.exp(-gate_ref[0, w, h : h + 1])) for w in range(2)
+            )
+            mixed = sacc[h] * (first / jnp.maximum(stot[h], 1.0)) + acc[h] * (
+                second / total[h]
             )
             mean = jnp.sum(mixed * mixed, 0, keepdims=True) * (1.0 / DH)
             both.append(mixed * lax.rsqrt(mean + EPS))
@@ -350,7 +386,7 @@
     rows = qblocks * groups
     width = groups * DH
     cosine, sine = rope_table(lax.axis_index("kv") * length, length)
-    gates = jax.nn.sigmoid(gate_logits[0]).transpose(0, 2, 1)
+    gates = gate_logits.transpose(0, 1, 3, 2)
     bf16, f32, i32 = jnp.bfloat16, jnp.float32, jnp.int32
     vm, dma = pltpu.VMEM, pltpu.SemaphoreType.DMA
     scratch = [

time: 29.5 us -> 24.5 us (0.83)
  Pallas kernels: 25.5 us -> 19.8 us
  local copies, waits for them, and re-layouts: 2.23 us -> 3.74 us
  other arithmetic: 1.34 us -> 0.55 us
    pallas_call x1, Pallas kernels: 25.5 us -> 19.8 us  [per_device(): pl.pallas_call(functools.partial(kernel, n), out_shape=jax.ShapeDtypeStru...]
    unnamed x15 -> x17, local copies, waits for them, and re-layouts: 2.23 us -> 3.74 us
    transpose x1 -> x0, other arithmetic: 0.79 us -> none  [per_device(): gates = jax.nn.sigmoid(gate_logits[0]).transpose(0, 2, 1)]
where the time goes in v2:
time: 24.5 us; the launch traced here: 24.2 us
  Pallas kernels  19.8 us (81%)
  local copies, waits for them, and re-layouts  3.74 us (15%)
  other arithmetic  0.55 us (2%)
    pallas_call x1, Pallas kernels, per_device(): pl.pallas_call(functools.partial(kernel, n), out_shape=jax.ShapeDtypeStru...  19.8 us
    unnamed x17, local copies, waits for them, and re-layouts  3.74 us
    mul x1, other arithmetic, rope_table(): return (jnp.cos(angle), jnp.sin(angle) * sign[None, :])  0.53 us

profile of v2, /device:TPU:24, one launch (start us, length us, event | category | flops | bytes accessed | tf_op | source)
XLA Modules:
  0.0 24.2 jit_solution(11240543915239513242)
XLA Ops:
  0.0 0.0 copy-start.7
  0.0 0.0 copy-start.6
  0.0 0.0 copy-start.4
  0.0 0.0 copy-start.1
  0.0 0.0 copy-start.2
  0.1 0.5 %fusion = (f32[256,128]{1,0:T(8,128)S(1)}, f32[256,128]{1,0:T(8,128)S(1)}) fusion(f32[128]{0:T(128)S(1)} %get-tuple-element.7, f32[128]{0:T(128)S(1)} %get-tuple-element.8, f32[256]{0:T(256)S(1)} %add_convert_fusion), kind=kLoop, calls=%fused_computation.2 | loop fusion | flops 65536 | bytes 264192 | tf_op jit(solution)/shard_map/mul | solution.py:29
  0.6 0.1 copy-done.7
  0.7 0.0 copy-done.6
  0.7 0.0 copy-done.4
  0.8 0.2 copy-done.1
  1.0 0.1 copy-done.2
  1.0 0.0 copy-start
  1.0 1.0 %copy-done = bf16[1,256,1024]{2,1,0:T(8,128)(2,1)S(1)} copy-done((bf16[1,256,1024]{2,1,0:T(8,128)(2,1)S(1)}, bf16[1,256,1024]{2,1,0:T(8,128)(2,1)}, u32[]{:S(2)}) %copy-start) | copy-done | bytes 524312
  2.1 0.0 copy-start.3
  2.1 0.8 %copy-done.3 = f32[1,2,256,16]{2,3,1,0:T(8,128)S(1)} copy-done((f32[1,2,256,16]{2,3,1,0:T(8,128)S(1)}, f32[1,2,256,16]{2,3,1,0:T(8,128)}, u32[]{:S(2)}) %copy-start.3) | copy-done | bytes 32792
  2.8 0.0 copy-start.5
  2.8 0.7 %copy-done.5 = f32[32,64]{1,0:T(8,128)S(1)} copy-done((f32[32,64]{1,0:T(8,128)S(1)}, f32[32,64]{1,0:T(8,128)}, u32[]{:S(2)}) %copy-start.5) | copy-done | bytes 8216
  3.5 19.8 %shard_map.82 = bf16[1,256,1024]{2,1,0:T(8,128)(2,1)S(1)} custom-call(bf16[1,256,1024]{2,1,0:T(8,128)(2,1)S(1)} %copy-done, bf16[1,256,256]{2,1,0:T(8,128)(2,1)S(1)} %copy-done.1, bf16[1,256,256]{2,1,0:T(8,128)(2,1)S(1)} %copy-done.2, f32[1,2,16,256]{3,2,1,0:T(8,128)S(1)} %bitcast.2, s32[1,2,4,16]{3,2,1,0:T(4,128)S(1)} %copy-done.6, f32[32,64]{1,0:T(8,128)S(1)} %copy-done.4, ...), custom_call_target="tpu_custom_call" | custom-call | tf_op jit(solution)/shard_map/pallas_call | solution.py:421
  23.4 0.8 %copy.10 = bf16[1,256,1024]{2,1,0:T(8,128)(2,1)} copy(bf16[1,256,1024]{2,1,0:T(8,128)(2,1)S(1)} %shard_map.82) | data formatting | bytes 1048576
  (2 shorter events, 0.0 us)
Async XLA Ops:
  0.0 0.7 %copy-start.7 = (f32[1024]{0:T(1024)S(1)}, f32[1024]{0:T(1024)}, u32[]{:S(2)}) copy-start(f32[1024]{0:T(1024)} %param.15) | copy-start | bytes 12292
  0.0 0.7 %copy-start.6 = (s32[1,2,4,16]{3,2,1,0:T(4,128)S(1)}, s32[1,2,4,16]{3,2,1,0:T(4,128)}, u32[]{:S(2)}) copy-start(s32[1,2,4,16]{3,2,1,0:T(4,128)} %list_ref.1) | copy-start | bytes 1540
  0.0 0.7 %copy-start.4 = (f32[32,64]{1,0:T(8,128)S(1)}, f32[32,64]{1,0:T(8,128)}, u32[]{:S(2)}) copy-start(f32[32,64]{1,0:T(8,128)} %pk_ref.1) | copy-start | bytes 24580
  0.0 0.9 %copy-start.1 = (bf16[1,256,256]{2,1,0:T(8,128)(2,1)S(1)}, bf16[1,256,256]{2,1,0:T(8,128)(2,1)}, u32[]{:S(2)}) copy-start(bf16[1,256,256]{2,1,0:T(8,128)(2,1)} %k_ref.1) | copy-start | bytes 393220
  0.0 1.0 %copy-start.2 = (bf16[1,256,256]{2,1,0:T(8,128)(2,1)S(1)}, bf16[1,256,256]{2,1,0:T(8,128)(2,1)}, u32[]{:S(2)}) copy-start(bf16[1,256,256]{2,1,0:T(8,128)(2,1)} %v_ref.1) | copy-start | bytes 393220
  1.0 1.0 %copy-start = (bf16[1,256,1024]{2,1,0:T(8,128)(2,1)S(1)}, bf16[1,256,1024]{2,1,0:T(8,128)(2,1)}, u32[]{:S(2)}) copy-start(bf16[1,256,1024]{2,1,0:T(8,128)(2,1)} %q_ref.1) | copy-start | bytes 1572868
  2.1 0.8 %copy-start.3 = (f32[1,2,256,16]{2,3,1,0:T(8,128)S(1)}, f32[1,2,256,16]{2,3,1,0:T(8,128)}, u32[]{:S(2)}) copy-start(f32[1,2,256,16]{2,3,1,0:T(8,128)} %param.11) | copy-start | bytes 98308
  2.8 0.7 %copy-start.5 = (f32[32,64]{1,0:T(8,128)S(1)}, f32[32,64]{1,0:T(8,128)}, u32[]{:S(2)}) copy-start(f32[32,64]{1,0:T(8,128)} %pv_ref.1) | copy-start | bytes 24580

commit v3 on v2

--- a/solution.py
+++ b/solution.py
@@ -2,6 +2,7 @@
 
 import jax
 import jax.numpy as jnp
+import numpy as np
 from jax import lax
 from jax.experimental import pallas as pl
 from jax.experimental.pallas import tpu as pltpu
@@ -20,13 +21,10 @@
 MESH = pl.DeviceIdType.MESH
 
 
-def rope_table(start, length):
+def frequencies():
     half = DH // 2
-    lane = jnp.arange(2 * DH)
-    freq = jnp.power(jnp.float32(THETA), -(2.0 * (lane % half).astype(jnp.float32)) / DH)
-    angle = (start + jnp.arange(length)).astype(jnp.float32)[:, None] * freq[None, :]
-    sign = jnp.where(lane % DH < half, -1.0, 1.0).astype(jnp.float32)
-    return jnp.cos(angle), jnp.sin(angle) * sign[None, :]
+    freq = np.power(np.float64(THETA), -(2.0 * (np.arange(2 * DH) % half)) / DH)
+    return np.broadcast_to(freq.astype(np.float32), (8, 2 * DH))
 
 
 def turn(x, cosine, sine):
@@ -37,9 +35,9 @@
 
 
 def kernel(
-    n, q_ref, k_ref, v_ref, gate_ref, list_ref, pk_ref, pv_ref, gain_ref, cos_ref, sin_ref,
+    n, q_ref, k_ref, v_ref, gate_ref, list_ref, pk_ref, pv_ref, gain_ref, freq_ref,
     out_ref,
-    qt, kt, vtl, kk, kkr, vtr, skk, svt, req, reqbuf, flag, own_bias, far_bias,
+    table, qt, kt, vtl, kk, kkr, vtr, skk, svt, req, reqbuf, flag, own_bias, far_bias,
     sumbuf, edge, sendk, sendv, recvk, recvv, bias,
     top, total, acc, stot, sacc,
     req_send, req_recv, sum_send, sum_recv, edge_send, edge_recv,
@@ -100,6 +98,13 @@
     for i in range(per):
         own_bias[i] = jnp.where(column(member, me * per + i) > 0.5, 0.0, NEG)
 
+    half = DH // 2
+    place = lax.broadcasted_iota(jnp.int32, (length, 2 * DH), 0) + me * length
+    angle = place.astype(f32) * freq_ref[:1]
+    sign = jnp.where(lax.broadcasted_iota(jnp.int32, (1, 2 * DH), 1) % DH < half, -1.0, 1.0)
+    table[0] = jnp.cos(angle)
+    table[1] = jnp.sin(angle) * sign
+
     pl.semaphore_wait(barrier, n - 1)
 
     def remote(src, dst, send, recv, peer, origin):
@@ -127,8 +132,8 @@
     def _(d):
         ask(me - 1 - d, me).start()
 
-    cosine = cos_ref[...]
-    sine = sin_ref[...]
+    cosine = table[0]
+    sine = table[1]
     low = lax.broadcasted_iota(jnp.int32, (length, 2 * DH), 1) < DH
     for p in range(slabs):
         cols = slice(p * 2 * DH, (p + 1) * 2 * DH)
@@ -385,11 +390,11 @@
     lanes = -(-total // 128) * 128
     rows = qblocks * groups
     width = groups * DH
-    cosine, sine = rope_table(lax.axis_index("kv") * length, length)
     gates = gate_logits.transpose(0, 1, 3, 2)
     bf16, f32, i32 = jnp.bfloat16, jnp.float32, jnp.int32
     vm, dma = pltpu.VMEM, pltpu.SemaphoreType.DMA
     scratch = [
+        vm((2, length, 2 * DH), f32),
         vm((heads // 2, length, 2 * DH), bf16),
         vm((length, width), bf16),
         vm((groups, DH, length), bf16),
@@ -421,13 +426,13 @@
     return pl.pallas_call(
         functools.partial(kernel, n),
         out_shape=jax.ShapeDtypeStruct(queries.shape, bf16),
-        in_specs=[pl.BlockSpec(memory_space=pltpu.VMEM)] * 10,
+        in_specs=[pl.BlockSpec(memory_space=pltpu.VMEM)] * 9,
         out_specs=pl.BlockSpec(memory_space=pltpu.VMEM),
         scratch_shapes=scratch,
         compiler_params=pltpu.CompilerParams(
             collective_id=0, has_side_effects=True, vmem_limit_bytes=48 << 20
         ),
-    )(queries, keys, values, gates, chosen, pool_k, pool_v, out_gain[None], cosine, sine)
+    )(queries, keys, values, gates, chosen, pool_k, pool_v, out_gain[None], jnp.asarray(frequencies()))
 
 
 def solution(mesh):

time: 24.5 us -> 26.8 us (1.094)
  local copies, waits for them, and re-layouts: 3.74 us -> 6.54 us
  other arithmetic: 0.55 us -> 0 us
    unnamed x17, local copies, waits for them, and re-layouts: 3.74 us -> 5.85 us
    another operation x0 -> x1, local copies, waits for them, and re-layouts: none -> 0.68 us
    mul x1 -> x0, other arithmetic: 0.53 us -> none  [rope_table(): return (jnp.cos(angle), jnp.sin(angle) * sign[None, :])]
where the time goes in v3:
time: 26.8 us; the launch traced here: 26.4 us
  Pallas kernels  19.8 us (74%)
  local copies, waits for them, and re-layouts  6.54 us (24%)
    pallas_call x1, Pallas kernels, per_device(): pl.pallas_call(functools.partial(kernel, n), out_shape=jax.ShapeDtypeStru...  19.8 us
    unnamed x17, local copies, waits for them, and re-layouts  5.85 us
    another operation x1, local copies, waits for them, and re-layouts  0.68 us

profile of v3, /device:TPU:24, one launch (start us, length us, event | category | flops | bytes accessed | tf_op | source)
XLA Modules:
  0.0 26.4 jit_solution(15467424410806339299)
XLA Ops:
  0.0 0.0 copy-start.7
  0.0 0.0 copy-start.6
  0.0 0.7 %jit_solution_.3.freq_ref = f32[8,128]{1,0:T(8,128)S(1)} broadcast(f32[128]{0:T(128)} %constant.2.clone), dimensions={1} | broadcast | bytes 4608 | tf_op jit(solution)
  0.7 0.0 copy-done.7
  0.7 0.0 copy-done.6
  0.7 0.0 copy-start
  0.7 1.0 %copy-done = bf16[1,256,1024]{2,1,0:T(8,128)(2,1)S(1)} copy-done((bf16[1,256,1024]{2,1,0:T(8,128)(2,1)S(1)}, bf16[1,256,1024]{2,1,0:T(8,128)(2,1)}, u32[]{:S(2)}) %copy-start) | copy-done | bytes 524312
  1.7 0.0 copy-start.1
  1.7 0.9 %copy-done.1 = bf16[1,256,256]{2,1,0:T(8,128)(2,1)S(1)} copy-done((bf16[1,256,256]{2,1,0:T(8,128)(2,1)S(1)}, bf16[1,256,256]{2,1,0:T(8,128)(2,1)}, u32[]{:S(2)}) %copy-start.1) | copy-done | bytes 131096
  2.7 0.0 copy-start.2
  2.7 0.9 %copy-done.2 = bf16[1,256,256]{2,1,0:T(8,128)(2,1)S(1)} copy-done((bf16[1,256,256]{2,1,0:T(8,128)(2,1)S(1)}, bf16[1,256,256]{2,1,0:T(8,128)(2,1)}, u32[]{:S(2)}) %copy-start.2) | copy-done | bytes 131096
  3.6 0.0 copy-start.3
  3.6 0.8 %copy-done.3 = f32[1,2,256,16]{2,3,1,0:T(8,128)S(1)} copy-done((f32[1,2,256,16]{2,3,1,0:T(8,128)S(1)}, f32[1,2,256,16]{2,3,1,0:T(8,128)}, u32[]{:S(2)}) %copy-start.3) | copy-done | bytes 32792
  4.3 0.0 copy-start.4
  4.3 0.7 %copy-done.4 = f32[32,64]{1,0:T(8,128)S(1)} copy-done((f32[32,64]{1,0:T(8,128)S(1)}, f32[32,64]{1,0:T(8,128)}, u32[]{:S(2)}) %copy-start.4) | copy-done | bytes 8216
  5.0 0.0 copy-start.5
  5.0 0.7 %copy-done.5 = f32[32,64]{1,0:T(8,128)S(1)} copy-done((f32[32,64]{1,0:T(8,128)S(1)}, f32[32,64]{1,0:T(8,128)}, u32[]{:S(2)}) %copy-start.5) | copy-done | bytes 8216
  5.7 19.8 %shard_map.91 = bf16[1,256,1024]{2,1,0:T(8,128)(2,1)S(1)} custom-call(bf16[1,256,1024]{2,1,0:T(8,128)(2,1)S(1)} %copy-done, bf16[1,256,256]{2,1,0:T(8,128)(2,1)S(1)} %copy-done.1, bf16[1,256,256]{2,1,0:T(8,128)(2,1)S(1)} %copy-done.2, f32[1,2,16,256]{3,2,1,0:T(8,128)S(1)} %bitcast.2, s32[1,2,4,16]{3,2,1,0:T(4,128)S(1)} %copy-done.6, f32[32,64]{1,0:T(8,128)S(1)} %copy-done.4, ...), custom_call_target="tpu_custom_call" | custom-call | tf_op jit(solution)/shard_map/pallas_call | solution.py:426
  25.6 0.8 %copy.11 = bf16[1,256,1024]{2,1,0:T(8,128)(2,1)} copy(bf16[1,256,1024]{2,1,0:T(8,128)(2,1)S(1)} %shard_map.91) | data formatting | bytes 1048576
Async XLA Ops:
  0.0 0.7 %copy-start.7 = (f32[1024]{0:T(1024)S(1)}, f32[1024]{0:T(1024)}, u32[]{:S(2)}) copy-start(f32[1024]{0:T(1024)} %param.16) | copy-start | bytes 12292
  0.0 0.7 %copy-start.6 = (s32[1,2,4,16]{3,2,1,0:T(4,128)S(1)}, s32[1,2,4,16]{3,2,1,0:T(4,128)}, u32[]{:S(2)}) copy-start(s32[1,2,4,16]{3,2,1,0:T(4,128)} %list_ref.1) | copy-start | bytes 1540
  0.7 1.0 %copy-start = (bf16[1,256,1024]{2,1,0:T(8,128)(2,1)S(1)}, bf16[1,256,1024]{2,1,0:T(8,128)(2,1)}, u32[]{:S(2)}) copy-start(bf16[1,256,1024]{2,1,0:T(8,128)(2,1)} %q_ref.1) | copy-start | bytes 1572868
  1.7 0.9 %copy-start.1 = (bf16[1,256,256]{2,1,0:T(8,128)(2,1)S(1)}, bf16[1,256,256]{2,1,0:T(8,128)(2,1)}, u32[]{:S(2)}) copy-start(bf16[1,256,256]{2,1,0:T(8,128)(2,1)} %k_ref.1) | copy-start | bytes 393220
  2.7 0.9 %copy-start.2 = (bf16[1,256,256]{2,1,0:T(8,128)(2,1)S(1)}, bf16[1,256,256]{2,1,0:T(8,128)(2,1)}, u32[]{:S(2)}) copy-start(bf16[1,256,256]{2,1,0:T(8,128)(2,1)} %v_ref.1) | copy-start | bytes 393220
  3.6 0.8 %copy-start.3 = (f32[1,2,256,16]{2,3,1,0:T(8,128)S(1)}, f32[1,2,256,16]{2,3,1,0:T(8,128)}, u32[]{:S(2)}) copy-start(f32[1,2,256,16]{2,3,1,0:T(8,128)} %param.12) | copy-start | bytes 98308
  4.3 0.7 %copy-start.4 = (f32[32,64]{1,0:T(8,128)S(1)}, f32[32,64]{1,0:T(8,128)}, u32[]{:S(2)}) copy-start(f32[32,64]{1,0:T(8,128)} %pk_ref.1) | copy-start | bytes 24580
  5.0 0.7 %copy-start.5 = (f32[32,64]{1,0:T(8,128)S(1)}, f32[32,64]{1,0:T(8,128)}, u32[]{:S(2)}) copy-start(f32[32,64]{1,0:T(8,128)} %pv_ref.1) | copy-start | bytes 24580
